TPU v7x, 32 devices: a whole 2x2x4 slice. The times are simulated.
32 devices in a mesh: ep: 8 (over z, y), tp: 4 (over x, core).
Axes of the slice: x: 2, y: 2, z: 4, core: 2. Of those that a mesh axis runs over, the one named last changes fastest.
Arguments:
- glu_value: bfloat16 [4096, 1024], P('ep', 'tp'), may hold values from -6 to 6
- glu_gate: bfloat16 [4096, 1024], P('ep', 'tp'), may hold values from -12 to 12
- conv_kernel: float32 [31, 1024], P(None, 'tp'), may hold values from -11.49474 to 11.49474
- ln_gain: float32 [1024], P('tp'), may hold values from 0.1 to 1.9
- out_weight: bfloat16 [1024, 2048], P('tp'), may hold values from -0.1875 to 0.1875
- moe_input: bfloat16 [2048, 2048], P('ep'), may hold values from -6 to 6
- moe_gain: float32 [2048], replicated, may hold values from 0.1 to 1.9
- gate_weight: bfloat16 [8, 2048, 3072], P('ep', None, 'tp'), may hold values from -0.125 to 0.125
- up_weight: bfloat16 [8, 2048, 3072], P('ep', None, 'tp'), may hold values from -0.125 to 0.125
- down_weight: bfloat16 [8, 3072, 2048], P('ep', 'tp'), may hold values from -0.109375 to 0.109375
- expert_ids: int32 [2048, 2], P('ep'), may hold values from 0 to 7, all different within a row; in each aligned block of 256 rows (0 to 255, 256 to 511, ...) at most 128 rows name the same one
- route_weight: float32 [2048, 2], P('ep'), may hold values from 0.2 to 1
Outputs:
- mixer_out: bfloat16 [4096, 2048], P(('ep', 'tp'))
- expert_out: bfloat16 [2048, 2048], P('ep', 'tp')
Inputs may be any that keep to these rules, and one draw needn't show every extreme that they name: `expert_ids`: each row names 2 different experts. In the rows of one device no expert is named by more than 128 rows; the bound is reached at some expert in some device's rows.
All inputs are finite; a program needn't handle non-finite values.
Results may differ from a plain program's by a relative error of at most 0.012.
Values may be sent and summed in bfloat16 or wider, within the bound.
A program may use at most 64 MiB of HBM per device.

v0:
```python
import jax
import jax.numpy as jnp
from jax import lax
from jax.sharding import PartitionSpec as P

eps_rms = 1e-06
eps_norm = 1e-05


def from_behind(value, axis, by):
    count = lax.axis_size(axis)
    pairs = [(i, i + by) for i in range(count) if 0 <= i + by < count]
    return lax.ppermute(value, axis, pairs)


def slot_numbers(expert_ids, experts, capacity):
    chosen = expert_ids.reshape(-1)
    onehot = (chosen[:, None] == jnp.arange(experts, dtype=jnp.int32)[None, :]).astype(jnp.int32)
    earlier = jnp.cumsum(onehot, axis=0) - onehot
    position = jnp.sum(earlier * onehot, axis=1)
    return chosen * capacity + position


def fill_slots(normed, slot_index, experts, capacity, chosen_per_token):
    owners = jnp.full((experts * capacity,), -1, jnp.int32)
    token_of = jnp.arange(slot_index.shape[0], dtype=jnp.int32) // chosen_per_token
    owners = owners.at[slot_index].set(token_of)
    picked = jnp.take(normed, jnp.maximum(owners, 0), axis=0)
    filled = jnp.where((owners >= 0)[:, None], picked, jnp.zeros_like(picked))
    return filled.reshape(experts, capacity, normed.shape[1])


def on_device(
    glu_value,
    glu_gate,
    conv_kernel,
    ln_gain,
    out_weight,
    moe_input,
    moe_gain,
    gate_weight,
    up_weight,
    down_weight,
    expert_ids,
    route_weight,
):
    length, channels_dev = glu_value.shape
    reach = conv_kernel.shape[0]
    tp_count = lax.axis_size("tp")
    gated = (glu_value.astype(jnp.float32) * jax.nn.sigmoid(glu_gate.astype(jnp.float32))).astype(
        jnp.bfloat16
    )
    earlier_rows = from_behind(gated[length - (reach - 1) :], "ep", 1)
    padded = jnp.concatenate([earlier_rows, gated], axis=0).astype(jnp.float32)
    convolved = jnp.zeros((length, channels_dev), jnp.float32)
    for tap_index in range(reach):
        begin = reach - 1 - tap_index
        convolved = convolved + conv_kernel[tap_index] * padded[begin : begin + length]
    total, squares = lax.psum(
        (jnp.sum(convolved, axis=1), jnp.sum(convolved * convolved, axis=1)), "tp"
    )
    channels = channels_dev * tp_count
    mean = total / channels
    variance = squares / channels - mean * mean
    scaled = (convolved - mean[:, None]) * lax.rsqrt(variance + eps_norm)[:, None] * ln_gain
    activated = jax.nn.silu(scaled).astype(jnp.bfloat16)
    mixer_out = lax.psum_scatter(
        jnp.dot(activated, out_weight, preferred_element_type=jnp.float32).astype(jnp.bfloat16),
        "tp",
        scatter_dimension=0,
        tiled=True,
    )
    tokens, model_width = moe_input.shape
    chosen_per_token = expert_ids.shape[1]
    experts = lax.axis_size("ep")
    capacity = 4 * max(1, tokens // experts)
    values = moe_input.astype(jnp.float32)
    normed = (
        values * lax.rsqrt(jnp.mean(values * values, axis=1, keepdims=True) + eps_rms) * moe_gain
    ).astype(jnp.bfloat16)
    slot_index = slot_numbers(expert_ids, experts, capacity)
    outgoing = fill_slots(normed, slot_index, experts, capacity, chosen_per_token)
    w_gate = gate_weight[0]
    w_up = up_weight[0]
    w_down = down_weight[0]
    quarter_slots = capacity // tp_count
    own_slots = lax.dynamic_slice_in_dim(
        outgoing, lax.axis_index("tp") * quarter_slots, quarter_slots, 1
    )
    arrived_part = lax.all_to_all(own_slots, "ep", split_axis=0, concat_axis=0, tiled=True)
    arrived = lax.all_gather(arrived_part, "tp", axis=1, tiled=True)
    flattened = arrived.reshape(-1, model_width)
    gate_act = jnp.dot(flattened, w_gate, preferred_element_type=jnp.float32)
    up_act = jnp.dot(flattened, w_up, preferred_element_type=jnp.float32)
    hidden_rows = (jax.nn.silu(gate_act) * up_act).astype(jnp.bfloat16)
    hidden = hidden_rows.reshape(arrived.shape[0], arrived.shape[1], w_gate.shape[1])
    sources = hidden.shape[0]
    partial_sum = jnp.dot(
        hidden.reshape(-1, hidden.shape[2]), w_down, preferred_element_type=jnp.float32
    )
    partial_sum = partial_sum.reshape(sources, capacity, model_width)
    answers = lax.psum_scatter(
        partial_sum.astype(jnp.bfloat16), "tp", scatter_dimension=2, tiled=True
    )
    returned = lax.all_to_all(answers, "ep", split_axis=0, concat_axis=0, tiled=True)
    feature_dev = returned.shape[2]
    picked = jnp.take(returned.reshape(experts * capacity, feature_dev), slot_index, axis=0)
    picked = picked.astype(jnp.float32).reshape(tokens, chosen_per_token, feature_dev)
    expert_out = jnp.sum(picked * route_weight[:, :, None], axis=1).astype(jnp.bfloat16)
    return (mixer_out, expert_out)


def solution(mesh):
    in_specs = (
        P("ep", "tp"),
        P("ep", "tp"),
        P(None, "tp"),
        P("tp"),
        P("tp", None),
        P("ep", None),
        P(),
        P("ep", None, "tp"),
        P("ep", None, "tp"),
        P("ep", "tp", None),
        P("ep", None),
        P("ep", None),
    )
    out_specs = (P(("ep", "tp"), None), P("ep", "tp"))
    return jax.shard_map(
        on_device, mesh=mesh, in_specs=in_specs, out_specs=out_specs, check_vma=False
    )
```

profile of v0, /device:TPU:0, one launch (start us, length us, event | category | flops | bytes accessed | tf_op | source)
XLA Modules:
  0.0 203.3 jit_solution(14986476686233676202)
XLA Ops:
  7.2 0.0 copy-start
  7.2 0.0 all-gather.2.cloned.1.call-start
  7.2 1.0 copy.20
  8.2 0.1 eq.26
  8.3 0.1 reshape.105
  8.5 0.7 broadcast_multiply_fusion
  9.2 1.1 reduce-window.6
  10.3 0.2 slice_reduce_fusion
  10.6 0.1 copy.24
  10.7 0.1 mul.502
  10.9 0.1 fusion.46
  11.0 2.4 %scatter_custom_fusion = s32[1024]{0:T(1024)S(1)} fusion(s32[512]{0:T(512)S(1)} %bitcast.67, s32[512]{0:T(512)S(1)} %add_select_fusion, s32[]{:T(128)} %constant.76.clone.1), kind=kCustom, calls=%fused_computation.109 | custom fusion | bytes 4100 | tf_op jit(solution)/shard_map/scatter | solution.py:27
  13.5 1.5 fusion.7
  15.0 2.5 %fusion.9 = bf16[256,2048]{1,0:T(8,128)(2,1)} fusion(bf16[256,2048]{1,0:T(8,128)(2,1)} %param.17, f32[2048]{0:T(1024)} %param.18, f32[256]{0:T(256)S(1)} %add_rsqrt_fusion.1), kind=kLoop, calls=%fused_computation.15 | loop fusion | flops 2097152 | bytes 2106368 | tf_op jit(solution)/shard_map/convert_element_type | solution.py:80
  17.5 10.2 %gather_fusion = bf16[1024,2048]{1,0:T(8,128)(2,1)} fusion(bf16[256,2048]{1,0:T(8,128)(2,1)} %fusion.9, s32[1024]{0:T(1024)S(1)} %maximum_clamp_fusion), kind=kCustom, calls=%fused_computation | custom fusion | bytes 8392704 | tf_op jit(solution)/shard_map/jit(_take)/gather | solution.py:28
  27.7 0.1 constant_dynamic-slice_fusion
  27.8 1.5 fusion.10
  29.3 33.0 %all_to_all.10 = bf16[8,32,2048]{2,1,0:T(8,128)(2,1)} all-to-all(bf16[8,32,2048]{2,1,0:T(8,128)(2,1)S(1)} %fusion.10), channel_id=1, replica_groups=mesh['ep'=8,'tp'=4] {'ep'}, dimensions={0} | all-to-all | bytes 2097152 | tf_op jit(solution)/shard_map/all_to_all | solution.py:90
  62.3 0.0 all-gather.2.cloned.1.call-update
  62.3 0.0 reduce-scatter.5.cloned.1.call-start
  62.4 33.6 %all-gather.2.cloned.1.call-done = bf16[8,128,2048]{2,1,0:T(8,128)(2,1)} async-done(((bf16[8,32,2048]{2,1,0:T(8,128)(2,1)}), bf16[8,128,2048]{2,1,0:T(8,128)(2,1)}) %all-gather.2.cloned.1.call-update) | async-done | bytes 4194320 | tf_op jit(solution)/shard_map/all_gather | solution.py:91
  95.9 0.0 copy-start.5
  95.9 0.0 copy-start.6
  95.9 6.3 %fusion.1 = f32[1024,768]{1,0:T(8,128)S(1)} fusion(bf16[1024,2048]{1,0:T(8,128)(2,1)} %bitcast.100, bf16[1,2048,768]{2,1,0:T(8,128)(2,1)} %param.20), kind=kOutput, calls=%fused_computation.5 | convolution fusion | flops 3221225472 | bytes 10485760 | tf_op jit(solution)/shard_map/dot_general | solution.py:94
  102.2 0.0 copy-done.5
  102.2 0.0 copy-done.6
  102.2 3.7 %multiply_convert_fusion = bf16[1024,768]{1,0:T(8,128)(2,1)S(1)} fusion(f32[1024,768]{1,0:T(8,128)S(1)} %fusion.1, bf16[1024,2048]{1,0:T(8,128)(2,1)S(1)} %bitcast.101, bf16[1,2048,768]{2,1,0:T(8,128)(2,1)S(1)} %copy-done.6), kind=kOutput, calls=%fused_computation.9 | convolution fusion | flops 3225944064 | bytes 12058624 | tf_op jit(solution)/shard_map/dot_general | solution.py:93
  106.0 0.0 copy-done
  106.0 5.0 %convolution_convert_fusion = bf16[8,128,2048]{2,1,0:T(8,128)(2,1)} fusion(bf16[8,128,768]{2,1,0:T(8,128)(2,1)S(1)} %bitcast.102, bf16[1,768,2048]{2,1,0:T(8,128)(2,1)S(1)} %copy-done), kind=kOutput, calls=%fused_computation.3 | convolution fusion | flops 3223322624 | bytes 8912896 | tf_op jit(solution)/shard_map/dot_general | solution.py:98
  110.9 0.0 copy-start.1
  110.9 0.0 copy-start.2
  110.9 0.0 reduce-scatter.5.cloned.1.call-update
  111.0 0.0 reduce-scatter.3.cloned.1.call-start
  111.0 0.9 copy-done.1
  111.9 1.1 multiply_convert_fusion.2
  113.0 3.4 %collective-permute-start = (bf16[30,256]{1,0:T(8,128)(2,1)S(1)}, bf16[30,256]{1,0:T(8,128)(2,1)S(1)}, u32[]{:S(2)}, u32[]{:S(2)}) collective-permute-start(bf16[30,256]{1,0:T(8,128)(2,1)S(1)} %slice.264), channel_id=1, source_target_pairs={{0,4},{4,8},{8,12},{12,16},{16,20},{20,24},{24,28},{1,5},{5,9},{9,... | collective-permute-start | bytes 46088 | tf_op jit(solution)/shard_map/ppermute | solution.py:13
  116.4 0.0 copy-done.2
  116.5 1.4 collective-permute-done
  117.8 0.1 maximum_convert_fusion
  117.9 0.0 copy-start.7
  117.9 2.9 %fusion.54 = (f32[512]{0:T(512)S(1)}, f32[512]{0:T(512)S(1)}, f32[512,256]{1,0:T(8,128)}) fusion(f32[542,256]{1,0:T(8,128)S(1)} %maximum_convert_fusion, f32[256]{0:T(256)S(1)} %bitcast.98, f32[256]{0:T(256)S(1)} %bitcast.99, f32[256]{0:T(256)S(1)} %bitcast.70, f32[256]{0:T(256)S(1)} %bitcast.71, f32[256]{0:T(256)S(1)} %bitcast.72, f32[256]{0:T(256)S(1)} %bitcast.73, ...), kind=kLoop, calls=%fused_computation.119 | loop fusion | flops 8387584 | bytes 16813056 | tf_op jit(solution)/shard_map/reduce_sum | solution.py:60
  120.8 6.1 %all-reduce = (f32[512]{0:T(512)S(1)}, f32[512]{0:T(512)S(1)}) all-reduce(f32[512]{0:T(512)S(1)} %get-tuple-element.3, f32[512]{0:T(512)S(1)} %get-tuple-element.2), channel_id=1, replica_groups=mesh['ep'=8,'tp'=4] {'tp'}, use_global_device_ids=true, to_apply=%region_3.0 | all-reduce | flops 1024 | bytes 8192 | tf_op jit(solution)/shard_map/psum | solution.py:59
  126.9 0.0 copy-done.7
  126.9 3.5 %convolution_convert_fusion.1 = bf16[512,2048]{1,0:T(8,128)(2,1)} fusion(bf16[256,2048]{1,0:T(8,128)(2,1)} %param.16, f32[512,256]{1,0:T(8,128)} %get-tuple-element.6, f32[256]{0:T(256)S(1)} %copy-done.7, f32[512]{0:T(512)S(1)} %get-tuple-element.41, f32[512]{0:T(512)S(1)} %get-tuple-element.40), kind=kOutput, calls=%fused_computation.10 | convolution fusion | flops 538968064 | bytes 3675136 | tf_op jit(solution)/shard_map/dot_general | solution.py:68
  130.5 0.0 copy-start.3
  130.5 0.0 copy-start.4
  130.5 0.0 reduce-scatter.3.cloned.1.call-update
  130.5 25.0 %reduce-scatter.5.cloned.1.call-done = bf16[8,128,512]{2,1,0:T(8,128)(2,1)} async-done(((bf16[8,128,2048]{2,1,0:T(8,128)(2,1)}), bf16[8,128,512]{2,1,0:T(8,128)(2,1)}) %reduce-scatter.5.cloned.1.call-update) | async-done | bytes 1048592 | tf_op jit(solution)/shard_map/reduce_scatter | solution.py:102
  155.5 5.5 %all-to-all-start.1 = ((bf16[8,128,512]{2,1,0:T(8,128)(2,1)}), bf16[8,128,512]{2,1,0:T(8,128)(2,1)}, u32[]{:S(2)}, u32[]{:S(2)}) async-start(bf16[8,128,512]{2,1,0:T(8,128)(2,1)} %reduce-scatter.5.cloned.1.call-done), calls=%async_computation.3 | async-start | bytes 2097152 | tf_op jit(solution)/shard_map/all_to_all | solution.py:105
  161.0 0.1 reduce_sum.52
  161.2 0.1 copy.22
  161.3 0.0 copy-done.3
  161.3 0.2 copy.23
  161.5 0.0 copy-done.4
  161.5 0.1 copy.25
  161.6 25.2 %all-to-all-done.1 = bf16[8,128,512]{2,1,0:T(8,128)(2,1)} async-done(((bf16[8,128,512]{2,1,0:T(8,128)(2,1)}), bf16[8,128,512]{2,1,0:T(8,128)(2,1)}, u32[]{:S(2)}, u32[]{:S(2)}) %all-to-all-start.1) | async-done | bytes 1048608 | tf_op jit(solution)/shard_map/all_to_all | solution.py:105
  186.8 4.0 %gather_fusion.1 = bf16[512,512]{1,0:T(8,128)(2,1)} fusion(bf16[1024,512]{1,0:T(8,128)(2,1)} %bitcast.44, s32[1024]{0:T(1024)S(1)} %pad_clamp_fusion), kind=kCustom, calls=%fused_computation.1 | custom fusion | bytes 1050624 | tf_op jit(solution)/shard_map/jit(_take)/gather | solution.py:107
  190.8 2.0 gather.15
  192.9 3.9 %multiply_reduce_fusion = bf16[256,512]{1,0:T(8,128)(2,1)} fusion(bf16[256,2,512]{2,1,0:T(2,128)(2,1)} %gather.15, pred[256,2]{1,0:T(8,128)(4,1)S(1)} %copy.23, f32[256,2]{1,0:T(8,128)S(1)} %copy.25), kind=kLoop, calls=%fused_computation.18 | loop fusion | flops 917504 | bytes 788992 | tf_op jit(solution)/shard_map/reduce_sum | solution.py:109
  196.7 0.0 reduce-scatter.3.cloned.1.call-done
  (14 shorter events, 0.2 us)
Async XLA Ops:
  7.2 98.8 %copy-start = (bf16[1,768,2048]{2,1,0:T(8,128)(2,1)S(1)}, bf16[1,768,2048]{2,1,0:T(8,128)(2,1)}, u32[]{:S(2)}) copy-start(bf16[1,768,2048]{2,1,0:T(8,128)(2,1)} %param.21) | copy-start | bytes 9437188
  7.2 88.8 %all-gather.2.cloned.1.call-start = ((), (), s32[]{:S(2)}) async-start(), calls=%async_computation.5 | async-start | bytes 5242880 | tf_op jit(solution)/shard_map/all_gather | solution.py:91
  62.3 93.2 %reduce-scatter.5.cloned.1.call-start = ((), (), s32[]{:S(2)}) async-start(), calls=%async_computation.6 | async-start | bytes 5242880 | tf_op jit(solution)/shard_map/reduce_scatter | solution.py:102
  95.9 6.3 %copy-start.5 = (bf16[8,128,2048]{2,1,0:T(8,128)(2,1)S(1)}, bf16[8,128,2048]{2,1,0:T(8,128)(2,1)}, u32[]{:S(2)}) copy-start(bf16[8,128,2048]{2,1,0:T(8,128)(2,1)} %all-gather.2.cloned.1.call-done) | copy-start | bytes 12582916
  95.9 6.3 %copy-start.6 = (bf16[1,2048,768]{2,1,0:T(8,128)(2,1)S(1)}, bf16[1,2048,768]{2,1,0:T(8,128)(2,1)}, u32[]{:S(2)}) copy-start(bf16[1,2048,768]{2,1,0:T(8,128)(2,1)} %param.19) | copy-start | bytes 9437188
  110.9 0.9 copy-start.1
  110.9 5.5 %copy-start.2 = (f32[31,256]{1,0:T(8,128)S(1)}, f32[31,256]{1,0:T(8,128)}, u32[]{:S(2)}) copy-start(f32[31,256]{1,0:T(8,128)} %param.14) | copy-start | bytes 95236
  111.0 85.8 %reduce-scatter.3.cloned.1.call-start = ((), (), s32[]{:S(2)}) async-start(), calls=%async_computation.4 | async-start | bytes 2621440 | tf_op jit(solution)/shard_map/reduce_scatter | solution.py:67
  113.0 4.8 %collective-permute-start = (bf16[30,256]{1,0:T(8,128)(2,1)S(1)}, bf16[30,256]{1,0:T(8,128)(2,1)S(1)}, u32[]{:S(2)}, u32[]{:S(2)}) collective-permute-start(bf16[30,256]{1,0:T(8,128)(2,1)S(1)} %slice.264), channel_id=1, source_target_pairs={{0,4},{4,8},{8,12},{12,16},{16,20},{20,24},{24,28},{1,5},{5,9},{9,... | collective-permute-start | bytes 46088 | tf_op jit(solution)/shard_map/ppermute | solution.py:13
  117.9 9.0 %copy-start.7 = (f32[256]{0:T(256)S(1)}, f32[256]{0:T(256)}, u32[]{:S(2)}) copy-start(f32[256]{0:T(256)} %param.15) | copy-start | bytes 3076
  130.5 30.8 %copy-start.3 = (s32[256,2]{0,1:T(2,128)S(1)}, s32[256,2]{0,1:T(2,128)}, u32[]{:S(2)}) copy-start(s32[256,2]{0,1:T(2,128)} %param.22) | copy-start | bytes 6148
  130.5 31.0 %copy-start.4 = (f32[256,2]{0,1:T(2,128)S(1)}, f32[256,2]{0,1:T(2,128)}, u32[]{:S(2)}) copy-start(f32[256,2]{0,1:T(2,128)} %param.23) | copy-start | bytes 6148
  155.5 31.3 %all-to-all-start.1 = ((bf16[8,128,512]{2,1,0:T(8,128)(2,1)}), bf16[8,128,512]{2,1,0:T(8,128)(2,1)}, u32[]{:S(2)}, u32[]{:S(2)}) async-start(bf16[8,128,512]{2,1,0:T(8,128)(2,1)} %reduce-scatter.5.cloned.1.call-done), calls=%async_computation.3 | async-start | bytes 2097152 | tf_op jit(solution)/shard_map/all_to_all | solution.py:105
Sparse Core Ops, SparseCore 0:
  62.4 33.4 all-gather.1
  111.1 44.3 reduce-scatter.4
  158.6 31.1 reduce-scatter.2
where the time goes:
time: 204 us; the launch traced here: 203 us
  waiting for transfers between devices  85.2 us (42%)
  blocking collectives  39.1 us (19%)
  local copies, waits for them, and re-layouts  22 us (11%)
  matrix products  18.5 us (9%)
  other arithmetic  15.5 us (8%)
  between operations  14 us (7%)
  starting transfers between devices  9.02 us (4%)
    all_gather x1, waiting for transfers between devices, on_device(): arrived = lax.all_gather(arrived_part, 'tp', axis=1, tiled=True)  33.6 us
    all_to_all x1, blocking collectives, on_device(): lax.all_to_all(own_slots, 'ep', split_axis=0, concat_axis=0, tiled=True)  33 us
    all_to_all x1, waiting for transfers between devices, on_device(): lax.all_to_all(answers, 'ep', split_axis=0, concat_axis=0, tiled=True)  25.2 us
    reduce_scatter x1, waiting for transfers between devices, on_device(): lax.psum_scatter(partial_sum.astype(jnp.bfloat16), 'tp', scatter_dimensio...  25 us
    gather x1, local copies, waits for them, and re-layouts, fill_slots(): picked = jnp.take(normed, jnp.maximum(owners, 0), axis=0)  10.2 us
    dot_general x1, matrix products, on_device(): up_act = jnp.dot(flattened, w_up, preferred_element_type=jnp.float32)  6.27 us
    psum x1, blocking collectives, on_device(): lax.psum((jnp.sum(convolved, axis=1), jnp.sum(convolved * convolved, axis...  6.09 us
    gather x2, local copies, waits for them, and re-layouts, on_device(): jnp.take(returned.reshape(experts * capacity, feature_dev), slot_index, a...  6.07 us
  transfers between devices with their start and end apart: 5, of which 4 were waited for; matrix products, arithmetic and copies ran while one was open for 9% of the time, Pallas kernels for 0%

commit v1 on v0

v1 whole, which is shorter than its diff:
```python
import functools

import jax
import jax.numpy as jnp
from jax import lax
from jax.experimental import pallas as pl
from jax.experimental.pallas import tpu as pltpu
from jax.sharding import PartitionSpec as P

eps_rms = 1e-06
eps_norm = 1e-05
MESH = pl.DeviceIdType.MESH
f32 = jnp.float32
bf16 = jnp.bfloat16


def kernel(
    n,
    tp,
    cap,
    group,
    reach,
    moe_ref,
    moe_gain_ref,
    ids_ref,
    ids_t_ref,
    route_ref,
    taps_ref,
    ln_gain_ref,
    value_hbm,
    gate_hbm,
    w_out_hbm,
    w_gate_hbm,
    w_up_hbm,
    w_down_hbm,
    mixer_ref,
    expert_ref,
    value,
    gate,
    w_out,
    w_gate,
    w_up,
    w_down,
    load_sem,
    slots,
    onehots,
    arrived,
    a2a_send,
    a2a_recv,
    fx_send,
    fx_recv,
    fp_send,
    fp_recv,
    fq_send,
    fq_recv,
    gated,
    halo_in,
    halo_send,
    halo_recv,
    padded,
    conv,
    stat_out,
    stat_in,
    stat_send,
    stat_recv,
    act,
    mix_out,
    mix_own,
    mix_in,
    mix_send,
    mix_recv,
    mix_x_out,
    mix_x_in,
    mix_x_send,
    mix_x_recv,
    rs_out,
    rs_own,
    rs_in,
    rs_send,
    rs_recv,
    rx_out,
    rx_in,
    rx_send,
    rx_recv,
    answer,
    returned,
    ret_send,
    ret_recv,
    total,
):
    me = lax.axis_index("ep")
    mine = lax.axis_index("tp")
    core = lax.rem(mine, 2)
    chip = mine // 2
    partner = chip * 2 + 1 - core
    chips = tp // 2
    groups = n // group
    rows = group * cap
    tokens, width = moe_ref.shape
    quarter = width // tp
    length, chan = value.shape
    halo = halo_in.shape[0]
    own_rows = length // tp

    def across(j):
        there = lax.rem(chip + j, chips)
        here = lax.rem(chip + chips - j, chips)
        return there * 2 + core, here * 2 + core

    barrier = pltpu.get_barrier_semaphore()

    def greet_ep(k, _):
        pl.semaphore_signal(
            barrier, inc=1, device_id={"ep": lax.rem(me + k, n)}, device_id_type=MESH
        )
        return 0

    lax.fori_loop(1, n, greet_ep, 0)
    for j in range(1, tp):
        pl.semaphore_signal(
            barrier, inc=1, device_id={"tp": lax.rem(mine + j, tp)}, device_id_type=MESH
        )

    loads = [
        pltpu.make_async_copy(src, dst, load_sem.at[i])
        for i, (src, dst) in enumerate(
            [
                (value_hbm, value),
                (gate_hbm, gate),
                (w_out_hbm, w_out),
                (w_gate_hbm.at[0], w_gate),
                (w_up_hbm.at[0], w_up),
                (w_down_hbm.at[0], w_down),
            ]
        )
    ]
    for load in loads:
        load.start()

    own_columns = pl.ds(pl.multiple_of(mine * quarter, 128), quarter)
    everything = moe_ref[...].astype(f32)
    inverse = lax.rsqrt(jnp.sum(everything * everything, axis=1, keepdims=True) / width + eps_rms)
    normed = (moe_ref[:, own_columns].astype(f32) * inverse * moe_gain_ref[:, own_columns]).astype(
        bf16
    )
    row = lax.broadcasted_iota(jnp.int32, (tokens, tokens), 0)
    col = lax.broadcasted_iota(jnp.int32, (tokens, tokens), 1)
    below = (col < row).astype(f32).astype(bf16)
    above = (row < col).astype(f32).astype(bf16)

    def a2a_copy(k):
        return pltpu.make_async_remote_copy(
            src_ref=slots.at[pl.ds(pl.multiple_of(k * cap, cap), cap)],
            dst_ref=arrived.at[mine, pl.ds(pl.multiple_of(k * cap, cap), cap)],
            send_sem=a2a_send.at[k],
            recv_sem=a2a_recv.at[k],
            device_id={"ep": lax.rem(me + k, n)},
            device_id_type=MESH,
        )

    def slot_rows(k):
        expert = lax.rem(me + k, n)
        member = jnp.maximum(
            (ids_t_ref[0:1, :] == expert).astype(f32), (ids_t_ref[1:2, :] == expert).astype(f32)
        )
        member = jnp.broadcast_to(member, (cap, tokens))
        place = jnp.dot(member.astype(bf16), above, preferred_element_type=f32)
        slot = lax.broadcasted_iota(jnp.int32, (cap, tokens), 0).astype(f32)
        pick = jnp.where(place == slot, member, 0.0).astype(bf16)
        return jnp.dot(pick, normed, preferred_element_type=f32).astype(bf16)

    own_slots = slot_rows(0)
    arrived[mine, 0:cap, :] = own_slots
    pl.semaphore_wait(barrier, n - 1 + tp - 1)

    def dispatch(k, _):
        slots[pl.ds(pl.multiple_of(k * cap, cap), cap), :] = slot_rows(k)
        a2a_copy(k).start()
        return 0

    lax.fori_loop(1, n, dispatch, 0)

    loads[0].wait()
    loads[1].wait()
    gated_now = (value[...].astype(f32) * jax.nn.sigmoid(gate[...].astype(f32))).astype(bf16)
    gated[...] = gated_now
    halo_copy = pltpu.make_async_remote_copy(
        src_ref=gated.at[pl.ds(length - halo, halo)],
        dst_ref=halo_in,
        send_sem=halo_send,
        recv_sem=halo_recv,
        device_id={"ep": lax.rem(me + 1, n)},
        device_id_type=MESH,
    )
    halo_copy.start()
    padded[pl.ds(halo, length), :] = gated_now.astype(f32)

    def place_of(k, _):
        expert = lax.rem(me + k, n)
        member = jnp.maximum(
            (ids_ref[:, 0:1] == expert).astype(f32), (ids_ref[:, 1:2] == expert).astype(f32)
        )
        member = jnp.broadcast_to(member, (tokens, cap))
        place = jnp.dot(below, member.astype(bf16), preferred_element_type=f32)
        slot = lax.broadcasted_iota(jnp.int32, (tokens, cap), 1).astype(f32)
        onehots[k] = jnp.where(place == slot, member, 0.0).astype(bf16)
        return 0

    lax.fori_loop(0, n, place_of, 0)

    def piece(ref, part, g):
        return ref.at[part, pl.ds(pl.multiple_of(g * rows, rows), rows)]

    def fx_copy(g, j):
        to, _ = across(j)
        return pltpu.make_async_remote_copy(
            src_ref=piece(arrived, mine, g),
            dst_ref=piece(arrived, mine, g),
            send_sem=fx_send.at[g, j - 1],
            recv_sem=fx_recv.at[g, j - 1],
            device_id={"tp": to},
            device_id_type=MESH,
        )

    def fp_copy(g):
        return pltpu.make_async_remote_copy(
            src_ref=piece(arrived, mine, g),
            dst_ref=piece(arrived, mine, g),
            send_sem=fp_send.at[g],
            recv_sem=fp_recv.at[g],
            device_id={"tp": partner},
            device_id_type=MESH,
        )

    def fq_copy(g, j):
        _, origin = across(j)
        return pltpu.make_async_remote_copy(
            src_ref=piece(arrived, origin, g),
            dst_ref=piece(arrived, origin, g),
            send_sem=fq_send.at[g, j - 1],
            recv_sem=fq_recv.at[g, j - 1],
            device_id={"tp": partner},
            device_id_type=MESH,
        )

    def forward_first(g):
        def arrival(k, _):
            @pl.when(k > 0)
            def _():
                a2a_copy(k).wait_recv()

            return 0

        lax.fori_loop(g * group, (g + 1) * group, arrival, 0)
        for j in range(1, chips):
            fx_copy(g, j).start()
        fp_copy(g).start()

    def forward_second(g):
        for j in range(1, chips):
            fx_copy(g, j).wait_recv()
            fq_copy(g, j).start()

    forward_first(0)

    halo_copy.wait_recv()
    padded[pl.ds(0, halo), :] = jnp.where(me == 0, 0.0, halo_in[...].astype(f32))
    step_rows = 64
    window = step_rows + halo

    for lane in range(0, chan, 128):

        def conv_step(i, _):
            base = pl.multiple_of(i * step_rows, step_rows)
            rows_in = padded[pl.ds(base, window), lane : lane + 128]
            result = jnp.zeros((step_rows, 128), f32)
            for shift in range(8):
                turned = rows_in if shift == 0 else pltpu.roll(rows_in, window - shift, 0)
                for tap in range(reach):
                    offset = halo - tap
                    if offset % 8 == shift:
                        begin = offset - shift
                        result = (
                            result
                            + taps_ref[tap : tap + 1, lane : lane + 128]
                            * turned[begin : begin + step_rows]
                        )
            conv[pl.ds(base, step_rows), lane : lane + 128] = result
            return 0

        lax.fori_loop(0, length // step_rows, conv_step, 0)

    convolved = conv[...]
    sums = jnp.sum(convolved, axis=1, keepdims=True)
    squares = jnp.sum(convolved * convolved, axis=1, keepdims=True)
    lanes = lax.broadcasted_iota(jnp.int32, (length, 128), 1)
    packed = jnp.where(lanes == 0, sums, jnp.where(lanes == 1, squares, 0.0))
    stat_out[...] = jnp.transpose(packed)[0:8]

    def stat_copy(j):
        return pltpu.make_async_remote_copy(
            src_ref=stat_out,
            dst_ref=stat_in.at[j - 1],
            send_sem=stat_send.at[j - 1],
            recv_sem=stat_recv.at[j - 1],
            device_id={"tp": lax.rem(mine + j, tp)},
            device_id_type=MESH,
        )

    for j in range(1, tp):
        stat_copy(j).start()

    if groups > 1:
        forward_first(1)
    forward_second(0)

    stats = stat_out[...]
    for j in range(1, tp):
        stat_copy(j).wait_recv()
        stats = stats + stat_in[j - 1]
    stats = jnp.concatenate([stats, jnp.zeros((120, length), f32)], axis=0)
    columns = jnp.transpose(stats)
    mean = columns[:, 0:1] / (chan * tp)
    variance = columns[:, 1:2] / (chan * tp) - mean * mean
    scaled = (conv[...] - mean) * lax.rsqrt(variance + eps_norm) * ln_gain_ref[...]
    act[...] = jax.nn.silu(scaled).astype(bf16)

    def mix_copy(xx):
        return pltpu.make_async_remote_copy(
            src_ref=mix_out.at[xx],
            dst_ref=mix_in.at[xx],
            send_sem=mix_send.at[xx],
            recv_sem=mix_recv.at[xx],
            device_id={"tp": partner},
            device_id_type=MESH,
        )

    def mix_part(owner):
        begin = pl.multiple_of(owner * own_rows, own_rows)
        return jnp.dot(act[pl.ds(begin, own_rows), :], w_out[...], preferred_element_type=f32)

    loads[2].wait()

    def mix_first(xx, _):
        mix_out[xx] = mix_part(xx * 2 + 1 - core).astype(bf16)
        mix_copy(xx).start()
        return 0

    def mix_second(xx, _):
        mix_own[xx] = mix_part(xx * 2 + core).astype(bf16)
        return 0

    lax.fori_loop(0, chips, mix_first, 0)
    lax.fori_loop(0, chips, mix_second, 0)

    def mix_x_copy(j):
        to, _ = across(j)
        return pltpu.make_async_remote_copy(
            src_ref=mix_x_out.at[j - 1],
            dst_ref=mix_x_in.at[j - 1],
            send_sem=mix_x_send.at[j - 1],
            recv_sem=mix_x_recv.at[j - 1],
            device_id={"tp": to},
            device_id_type=MESH,
        )

    def mix_stage():
        for xx in range(chips):
            mix_copy(xx).wait_recv()
        for j in range(1, chips):
            there = lax.rem(chip + j, chips)
            mix_x_out[j - 1] = (mix_own[there].astype(f32) + mix_in[there].astype(f32)).astype(
                bf16
            )
            mix_x_copy(j).start()

    loads[3].wait()
    loads[4].wait()
    loads[5].wait()

    def rs_copy(g, xx):
        return pltpu.make_async_remote_copy(
            src_ref=rs_out.at[g, xx],
            dst_ref=rs_in.at[g, xx],
            send_sem=rs_send.at[g, xx],
            recv_sem=rs_recv.at[g, xx],
            device_id={"tp": partner},
            device_id_type=MESH,
        )

    def rx_copy(g, j):
        to, _ = across(j)
        return pltpu.make_async_remote_copy(
            src_ref=rx_out.at[g, j - 1],
            dst_ref=rx_in.at[g, j - 1],
            send_sem=rx_send.at[g, j - 1],
            recv_sem=rx_recv.at[g, j - 1],
            device_id={"tp": to},
            device_id_type=MESH,
        )

    def ret_copy(k):
        return pltpu.make_async_remote_copy(
            src_ref=answer.at[pl.ds(pl.multiple_of(k * cap, cap), cap)],
            dst_ref=returned.at[pl.ds(pl.multiple_of(k * cap, cap), cap)],
            send_sem=ret_send.at[k],
            recv_sem=ret_recv.at[k],
            device_id={"ep": lax.rem(me + n - k, n)},
            device_id_type=MESH,
        )

    def expert_step(g):
        fp_copy(g).wait_recv()
        for j in range(1, chips):
            fq_copy(g, j).wait_recv()
        gate_act = jnp.zeros((rows, w_gate.shape[1]), f32)
        up_act = jnp.zeros((rows, w_up.shape[1]), f32)
        block = pl.ds(pl.multiple_of(g * rows, rows), rows)
        x = jnp.concatenate([arrived[part, block] for part in range(tp)], axis=1)
        gate_act = jnp.dot(x, w_gate[...], preferred_element_type=f32)
        up_act = jnp.dot(x, w_up[...], preferred_element_type=f32)
        hidden = (jax.nn.silu(gate_act) * up_act).astype(bf16)
        for xx in range(chips):
            begin = pl.multiple_of((xx * 2 + 1 - core) * quarter, 128)
            rs_out[g, xx] = jnp.dot(
                hidden, w_down[:, pl.ds(begin, quarter)], preferred_element_type=f32
            ).astype(bf16)
            rs_copy(g, xx).start()
        for xx in range(chips):
            begin = pl.multiple_of((xx * 2 + core) * quarter, 128)
            rs_own[g, xx] = jnp.dot(
                hidden, w_down[:, pl.ds(begin, quarter)], preferred_element_type=f32
            ).astype(bf16)

    def sum_step(g):
        for xx in range(chips):
            rs_copy(g, xx).wait_recv()
        for j in range(1, chips):
            there = lax.rem(chip + j, chips)
            rx_out[g, j - 1] = (rs_own[g, there].astype(f32) + rs_in[g, there].astype(f32)).astype(
                bf16
            )
            rx_copy(g, j).start()

    def return_step(g):
        result = rs_own[g, chip].astype(f32) + rs_in[g, chip].astype(f32)
        for j in range(1, chips):
            rx_copy(g, j).wait_recv()
            result = result + rx_in[g, j - 1].astype(f32)
        result = result.astype(bf16)
        answer[pl.ds(pl.multiple_of(g * rows, rows), rows), :] = result

        @pl.when(g == 0)
        def _():
            returned[0:cap, :] = result[0:cap]

        def give(k, _):
            @pl.when(k > 0)
            def _():
                ret_copy(k).start()

            return 0

        lax.fori_loop(g * group, (g + 1) * group, give, 0)

    total[...] = jnp.zeros_like(total)

    def combine_step(g):
        def take(k, _):
            @pl.when(k > 0)
            def _():
                ret_copy(k).wait_recv()

            expert = lax.rem(me + k, n)
            weight = jnp.where(ids_ref[:, 0:1] == expert, route_ref[:, 0:1], 0.0) + jnp.where(
                ids_ref[:, 1:2] == expert, route_ref[:, 1:2], 0.0
            )
            answers = returned[pl.ds(pl.multiple_of(k * cap, cap), cap), :]
            total[...] += weight * jnp.dot(onehots[k], answers, preferred_element_type=f32)
            return 0

        lax.fori_loop(g * group, (g + 1) * group, take, 0)

    def step(g, _):
        @pl.when(g + 2 < groups)
        def _():
            forward_first(g + 2)

        @pl.when(g + 1 < groups)
        def _():
            forward_second(g + 1)

        @pl.when(g < groups)
        def _():
            expert_step(g)

        @pl.when(g == 0)
        def _():
            mix_stage()

        @pl.when((g >= 1) & (g < groups + 1))
        def _():
            sum_step(g - 1)

        @pl.when((g >= 2) & (g < groups + 2))
        def _():
            return_step(g - 2)

        @pl.when(g >= 3)
        def _():
            combine_step(g - 3)

        return 0

    lax.fori_loop(0, groups + 3, step, 0)
    expert_ref[...] = total[...].astype(bf16)

    mixed = mix_own[chip].astype(f32) + mix_in[chip].astype(f32)
    for j in range(1, chips):
        mix_x_copy(j).wait_recv()
        mixed = mixed + mix_x_in[j - 1].astype(f32)
    mixer_ref[...] = mixed.astype(bf16)

    def left(k, _):
        a2a_copy(k).wait_send()
        ret_copy(k).wait_send()
        return 0

    lax.fori_loop(1, n, left, 0)
    halo_copy.wait_send()
    for j in range(1, tp):
        stat_copy(j).wait_send()
    for xx in range(chips):
        mix_copy(xx).wait_send()
    for j in range(1, chips):
        mix_x_copy(j).wait_send()

    def left_group(g, _):
        fp_copy(g).wait_send()
        for j in range(1, chips):
            fx_copy(g, j).wait_send()
            fq_copy(g, j).wait_send()
            rx_copy(g, j).wait_send()
        for xx in range(chips):
            rs_copy(g, xx).wait_send()
        return 0

    lax.fori_loop(0, groups, left_group, 0)


def on_device(
    glu_value,
    glu_gate,
    conv_kernel,
    ln_gain,
    out_weight,
    moe_input,
    moe_gain,
    gate_weight,
    up_weight,
    down_weight,
    expert_ids,
    route_weight,
):
    n = lax.axis_size("ep")
    tp = lax.axis_size("tp")
    chips = tp // 2
    length, chan = glu_value.shape
    reach = conv_kernel.shape[0]
    halo = -(-(reach - 1) // 16) * 16
    tokens, width = moe_input.shape
    hidden = gate_weight.shape[2]
    cap = 4 * max(1, tokens // n)
    group = max(1, min(n, 256 // cap))
    groups = n // group
    rows = group * cap
    quarter = width // tp
    own_rows = length // tp
    vmem = pl.BlockSpec(memory_space=pltpu.VMEM)
    hbm = pl.BlockSpec(memory_space=pl.ANY)
    dma = pltpu.SemaphoreType.DMA
    V = pltpu.VMEM
    others = max(1, chips - 1)
    return pl.pallas_call(
        functools.partial(kernel, n, tp, cap, group, reach),
        out_shape=(
            jax.ShapeDtypeStruct((own_rows, out_weight.shape[1]), bf16),
            jax.ShapeDtypeStruct((tokens, quarter), bf16),
        ),
        in_specs=[vmem] * 7 + [hbm] * 6,
        out_specs=(vmem, vmem),
        scratch_shapes=[
            V((length, chan), bf16),
            V((length, chan), bf16),
            V(out_weight.shape, bf16),
            V((width, hidden), bf16),
            V((width, hidden), bf16),
            V((hidden, width), bf16),
            dma((6,)),
            V((n * cap, quarter), bf16),
            V((n, tokens, cap), bf16),
            V((tp, n * cap, quarter), bf16),
            dma((n,)),
            dma((n,)),
            dma((groups, others)),
            dma((groups, others)),
            dma((groups,)),
            dma((groups,)),
            dma((groups, others)),
            dma((groups, others)),
            V((length, chan), bf16),
            V((halo, chan), bf16),
            dma,
            dma,
            V((length + halo, chan), f32),
            V((length, chan), f32),
            V((8, length), f32),
            V((tp - 1, 8, length), f32),
            dma((tp - 1,)),
            dma((tp - 1,)),
            V((length, chan), bf16),
            V((chips, own_rows, out_weight.shape[1]), bf16),
            V((chips, own_rows, out_weight.shape[1]), bf16),
            V((chips, own_rows, out_weight.shape[1]), bf16),
            dma((chips,)),
            dma((chips,)),
            V((others, own_rows, out_weight.shape[1]), bf16),
            V((others, own_rows, out_weight.shape[1]), bf16),
            dma((others,)),
            dma((others,)),
            V((groups, chips, rows, quarter), bf16),
            V((groups, chips, rows, quarter), bf16),
            V((groups, chips, rows, quarter), bf16),
            dma((groups, chips)),
            dma((groups, chips)),
            V((groups, others, rows, quarter), bf16),
            V((groups, others, rows, quarter), bf16),
            dma((groups, others)),
            dma((groups, others)),
            V((n * cap, quarter), bf16),
            V((n * cap, quarter), bf16),
            dma((n,)),
            dma((n,)),
            V((tokens, quarter), f32),
        ],
        compiler_params=pltpu.CompilerParams(
            collective_id=0, has_side_effects=True, vmem_limit_bytes=60 * 1024 * 1024
        ),
        name="block",
    )(
        moe_input,
        moe_gain.reshape(1, -1),
        expert_ids,
        expert_ids.T,
        route_weight,
        conv_kernel,
        ln_gain.reshape(1, -1),
        glu_value,
        glu_gate,
        out_weight,
        gate_weight,
        up_weight,
        down_weight,
    )


def solution(mesh):
    in_specs = (
        P("ep", "tp"),
        P("ep", "tp"),
        P(None, "tp"),
        P("tp"),
        P("tp", None),
        P("ep", None),
        P(),
        P("ep", None, "tp"),
        P("ep", None, "tp"),
        P("ep", "tp", None),
        P("ep", None),
        P("ep", None),
    )
    out_specs = (P(("ep", "tp"), None), P("ep", "tp"))
    return jax.shard_map(
        on_device, mesh=mesh, in_specs=in_specs, out_specs=out_specs, check_vma=False
    )
```

time: 204 us -> 107 us (0.52)
  the two profiles are of different devices: /device:TPU:0 before, /device:TPU:8 now
where the time goes in v1:
time: 107 us
  Pallas kernels  99.9 us (93%)
  local copies, waits for them, and re-layouts  6.5 us (6%)
    pallas_call x1, Pallas kernels, on_device(): pl.pallas_call(functools.partial(kernel, n, tp, cap, group, reach), out_s...  99.9 us
    unnamed x4, local copies, waits for them, and re-layouts  6.5 us

profile of v1, /device:TPU:8, one launch (start us, length us, event | category | flops | bytes accessed | tf_op | source)
XLA Modules:
  0.0 107.1 jit_solution(4475181956519498892)
XLA Ops:
  0.6 1.5 %copy.15.route_ref = f32[256,2]{1,0:T(8,128)} copy(f32[256,2]{0,1:T(2,128)} %param.23) | data formatting | bytes 4096 | tf_op args[11]
  2.1 1.5 %copy.14.ids_ref = s32[256,2]{1,0:T(8,128)} copy(s32[256,2]{0,1:T(2,128)} %param.22) | data formatting | bytes 4096 | tf_op args[10]
  3.6 99.9 %block.1 = (bf16[128,2048]{1,0:T(8,128)(2,1)}, bf16[256,512]{1,0:T(8,128)(2,1)}) custom-call(bf16[256,2048]{1,0:T(8,128)(2,1)} %moe_ref.1, f32[1,2048]{1,0:T(1,128)} %bitcast.3, s32[256,2]{1,0:T(8,128)} %copy.14.ids_ref, s32[2,256]{1,0:T(2,128)} %bitcast.4, f32[256,2]{1,0:T(8,128)} %copy.15.route_ref, f32[31,256]{1,0:T(8,128)} %taps_ref.1, ...), custom_call_target="tpu_custom_call" | custom-call | tf_op jit(solution)/shard_map/block/pallas_call | solution.py:584
  103.5 1.9 %copy.18 = bf16[128,2048]{1,0:T(8,128)(2,1)} copy(bf16[128,2048]{1,0:T(8,128)(2,1)} %get-tuple-element.4) | data formatting | bytes 1048576
  105.4 1.7 %copy.19 = bf16[256,512]{1,0:T(8,128)(2,1)} copy(bf16[256,512]{1,0:T(8,128)(2,1)} %get-tuple-element.5) | data formatting | bytes 524288

commit v2 on v1

--- a/solution.py
+++ b/solution.py
@@ -42,9 +42,15 @@
     w_up,
     w_down,
     load_sem,
+    normed,
     slots,
+    near_slots,
     onehots,
     arrived,
+    near_send,
+    near_recv,
+    fn_send,
+    fn_recv,
     a2a_send,
     a2a_recv,
     fx_send,
@@ -102,6 +108,18 @@
     halo = halo_in.shape[0]
     own_rows = length // tp
 
+    def toward(k):
+        return lax.rem(me // 2 + k // 2, n // 2) * 2 + lax.rem(me + k, 2)
+
+    def source(k):
+        return lax.rem(me // 2 + n // 2 - k // 2, n // 2) * 2 + lax.rem(me + k, 2)
+
+    def block(k):
+        return pl.ds(pl.multiple_of(k * cap, cap), cap)
+
+    def columns_of(part):
+        return pl.ds(pl.multiple_of(part * quarter, 128), quarter)
+
     def across(j):
         there = lax.rem(chip + j, chips)
         here = lax.rem(chip + chips - j, chips)
@@ -137,12 +155,9 @@
     for load in loads:
         load.start()
 
-    own_columns = pl.ds(pl.multiple_of(mine * quarter, 128), quarter)
     everything = moe_ref[...].astype(f32)
     inverse = lax.rsqrt(jnp.sum(everything * everything, axis=1, keepdims=True) / width + eps_rms)
-    normed = (moe_ref[:, own_columns].astype(f32) * inverse * moe_gain_ref[:, own_columns]).astype(
-        bf16
-    )
+    normed[...] = (everything * inverse * moe_gain_ref[...]).astype(bf16)
     row = lax.broadcasted_iota(jnp.int32, (tokens, tokens), 0)
     col = lax.broadcasted_iota(jnp.int32, (tokens, tokens), 1)
     below = (col < row).astype(f32).astype(bf16)
@@ -150,35 +165,51 @@
 
     def a2a_copy(k):
         return pltpu.make_async_remote_copy(
-            src_ref=slots.at[pl.ds(pl.multiple_of(k * cap, cap), cap)],
-            dst_ref=arrived.at[mine, pl.ds(pl.multiple_of(k * cap, cap), cap)],
+            src_ref=slots.at[block(k)],
+            dst_ref=arrived.at[mine, block(k)],
             send_sem=a2a_send.at[k],
             recv_sem=a2a_recv.at[k],
-            device_id={"ep": lax.rem(me + k, n)},
-            device_id_type=MESH,
-        )
-
-    def slot_rows(k):
-        expert = lax.rem(me + k, n)
+            device_id={"ep": toward(k)},
+            device_id_type=MESH,
+        )
+
+    def near_copy(xx):
+        return pltpu.make_async_remote_copy(
+            src_ref=near_slots.at[xx],
+            dst_ref=arrived.at[xx * 2 + core, pl.ds(cap, cap)],
+            send_sem=near_send.at[xx],
+            recv_sem=near_recv.at[xx],
+            device_id={"ep": toward(1)},
+            device_id_type=MESH,
+        )
+
+    def slot_picks(k):
+        expert = toward(k)
         member = jnp.maximum(
             (ids_t_ref[0:1, :] == expert).astype(f32), (ids_t_ref[1:2, :] == expert).astype(f32)
         )
         member = jnp.broadcast_to(member, (cap, tokens))
         place = jnp.dot(member.astype(bf16), above, preferred_element_type=f32)
         slot = lax.broadcasted_iota(jnp.int32, (cap, tokens), 0).astype(f32)
-        pick = jnp.where(place == slot, member, 0.0).astype(bf16)
-        return jnp.dot(pick, normed, preferred_element_type=f32).astype(bf16)
-
-    own_slots = slot_rows(0)
-    arrived[mine, 0:cap, :] = own_slots
+        return jnp.where(place == slot, member, 0.0).astype(bf16)
+
+    def picked(pick, part):
+        return jnp.dot(
+            pick, normed[:, columns_of(part)], preferred_element_type=f32
+        ).astype(bf16)
+
     pl.semaphore_wait(barrier, n - 1 + tp - 1)
 
     def dispatch(k, _):
-        slots[pl.ds(pl.multiple_of(k * cap, cap), cap), :] = slot_rows(k)
+        slots[block(k), :] = picked(slot_picks(k), mine)
         a2a_copy(k).start()
         return 0
 
-    lax.fori_loop(1, n, dispatch, 0)
+    lax.fori_loop(2, n, dispatch, 0)
+    pick = slot_picks(1)
+    for xx in range(chips):
+        near_slots[xx] = picked(pick, xx * 2 + core)
+        near_copy(xx).start()
 
     loads[0].wait()
     loads[1].wait()
@@ -195,73 +226,83 @@
     halo_copy.start()
     padded[pl.ds(halo, length), :] = gated_now.astype(f32)
 
-    def place_of(k, _):
-        expert = lax.rem(me + k, n)
-        member = jnp.maximum(
-            (ids_ref[:, 0:1] == expert).astype(f32), (ids_ref[:, 1:2] == expert).astype(f32)
-        )
-        member = jnp.broadcast_to(member, (tokens, cap))
-        place = jnp.dot(below, member.astype(bf16), preferred_element_type=f32)
-        slot = lax.broadcasted_iota(jnp.int32, (tokens, cap), 1).astype(f32)
-        onehots[k] = jnp.where(place == slot, member, 0.0).astype(bf16)
-        return 0
-
-    lax.fori_loop(0, n, place_of, 0)
-
-    def piece(ref, part, g):
-        return ref.at[part, pl.ds(pl.multiple_of(g * rows, rows), rows)]
-
-    def fx_copy(g, j):
+    pick = slot_picks(0)
+    for part in range(tp):
+        arrived[part, 0:cap, :] = picked(pick, part)
+
+    def fx_copy(k, j):
         to, _ = across(j)
         return pltpu.make_async_remote_copy(
-            src_ref=piece(arrived, mine, g),
-            dst_ref=piece(arrived, mine, g),
-            send_sem=fx_send.at[g, j - 1],
-            recv_sem=fx_recv.at[g, j - 1],
+            src_ref=arrived.at[mine, block(k)],
+            dst_ref=arrived.at[mine, block(k)],
+            send_sem=fx_send.at[k, j - 1],
+            recv_sem=fx_recv.at[k, j - 1],
             device_id={"tp": to},
             device_id_type=MESH,
         )
 
-    def fp_copy(g):
-        return pltpu.make_async_remote_copy(
-            src_ref=piece(arrived, mine, g),
-            dst_ref=piece(arrived, mine, g),
-            send_sem=fp_send.at[g],
-            recv_sem=fp_recv.at[g],
+    def fp_copy(k):
+        return pltpu.make_async_remote_copy(
+            src_ref=arrived.at[mine, block(k)],
+            dst_ref=arrived.at[mine, block(k)],
+            send_sem=fp_send.at[k],
+            recv_sem=fp_recv.at[k],
             device_id={"tp": partner},
             device_id_type=MESH,
         )
 
-    def fq_copy(g, j):
+    def fq_copy(k, j):
         _, origin = across(j)
         return pltpu.make_async_remote_copy(
-            src_ref=piece(arrived, origin, g),
-            dst_ref=piece(arrived, origin, g),
-            send_sem=fq_send.at[g, j - 1],
-            recv_sem=fq_recv.at[g, j - 1],
+            src_ref=arrived.at[origin, block(k)],
+            dst_ref=arrived.at[origin, block(k)],
+            send_sem=fq_send.at[k, j - 1],
+            recv_sem=fq_recv.at[k, j - 1],
             device_id={"tp": partner},
             device_id_type=MESH,
         )
 
+    def fn_copy(xx):
+        return pltpu.make_async_remote_copy(
+            src_ref=arrived.at[xx * 2 + core, pl.ds(cap, cap)],
+            dst_ref=arrived.at[xx * 2 + core, pl.ds(cap, cap)],
+            send_sem=fn_send.at[xx],
+            recv_sem=fn_recv.at[xx],
+            device_id={"tp": partner},
+            device_id_type=MESH,
+        )
+
+    def over_group(g, do, first=2):
+        def one(k, _):
+            @pl.when(k >= first)
+            def _():
+                do(k)
+
+            return 0
+
+        lax.fori_loop(g * group, (g + 1) * group, one, 0)
+
     def forward_first(g):
-        def arrival(k, _):
-            @pl.when(k > 0)
-            def _():
-                a2a_copy(k).wait_recv()
-
-            return 0
-
-        lax.fori_loop(g * group, (g + 1) * group, arrival, 0)
-        for j in range(1, chips):
-            fx_copy(g, j).start()
-        fp_copy(g).start()
+        def one(k):
+            a2a_copy(k).wait_recv()
+            for j in range(1, chips):
+                fx_copy(k, j).start()
+            fp_copy(k).start()
+
+        over_group(g, one)
 
     def forward_second(g):
-        for j in range(1, chips):
-            fx_copy(g, j).wait_recv()
-            fq_copy(g, j).start()
-
-    forward_first(0)
+        def one(k):
+            for j in range(1, chips):
+                fx_copy(k, j).wait_recv()
+                fq_copy(k, j).start()
+
+        over_group(g, one)
+
+    def forward_near():
+        for xx in range(chips):
+            near_copy(xx).wait_recv()
+            fn_copy(xx).start()
 
     halo_copy.wait_recv()
     padded[pl.ds(0, halo), :] = jnp.where(me == 0, 0.0, halo_in[...].astype(f32))
@@ -310,6 +351,8 @@
     for j in range(1, tp):
         stat_copy(j).start()
 
+    forward_near()
+    forward_first(0)
     if groups > 1:
         forward_first(1)
     forward_second(0)
@@ -353,13 +396,16 @@
     lax.fori_loop(0, chips, mix_first, 0)
     lax.fori_loop(0, chips, mix_second, 0)
 
-    def mix_x_copy(j):
+    half = own_rows // 2
+
+    def mix_x_copy(j, part):
         to, _ = across(j)
-        return pltpu.make_async_remote_copy(
-            src_ref=mix_x_out.at[j - 1],
-            dst_ref=mix_x_in.at[j - 1],
-            send_sem=mix_x_send.at[j - 1],
-            recv_sem=mix_x_recv.at[j - 1],
+        span = pl.ds(part * half, half)
+        return pltpu.make_async_remote_copy(
+            src_ref=mix_x_out.at[j - 1, span],
+            dst_ref=mix_x_in.at[j - 1, span],
+            send_sem=mix_x_send.at[j - 1, part],
+            recv_sem=mix_x_recv.at[j - 1, part],
             device_id={"tp": to},
             device_id_type=MESH,
         )
@@ -372,8 +418,6 @@
             mix_x_out[j - 1] = (mix_own[there].astype(f32) + mix_in[there].astype(f32)).astype(
                 bf16
             )
-            mix_x_copy(j).start()
-
     loads[3].wait()
     loads[4].wait()
     loads[5].wait()
@@ -388,35 +432,41 @@
             device_id_type=MESH,
         )
 
-    def rx_copy(g, j):
+    def rx_copy(k, j):
         to, _ = across(j)
         return pltpu.make_async_remote_copy(
-            src_ref=rx_out.at[g, j - 1],
-            dst_ref=rx_in.at[g, j - 1],
-            send_sem=rx_send.at[g, j - 1],
-            recv_sem=rx_recv.at[g, j - 1],
+            src_ref=rx_out.at[j - 1, block(k)],
+            dst_ref=rx_in.at[j - 1, block(k)],
+            send_sem=rx_send.at[k, j - 1],
+            recv_sem=rx_recv.at[k, j - 1],
             device_id={"tp": to},
             device_id_type=MESH,
         )
 
     def ret_copy(k):
         return pltpu.make_async_remote_copy(
-            src_ref=answer.at[pl.ds(pl.multiple_of(k * cap, cap), cap)],
-            dst_ref=returned.at[pl.ds(pl.multiple_of(k * cap, cap), cap)],
+            src_ref=answer.at[block(k)],
+            dst_ref=returned.at[block(k)],
             send_sem=ret_send.at[k],
             recv_sem=ret_recv.at[k],
-            device_id={"ep": lax.rem(me + n - k, n)},
+            device_id={"ep": source(k)},
             device_id_type=MESH,
         )
 
     def expert_step(g):
-        fp_copy(g).wait_recv()
-        for j in range(1, chips):
-            fq_copy(g, j).wait_recv()
-        gate_act = jnp.zeros((rows, w_gate.shape[1]), f32)
-        up_act = jnp.zeros((rows, w_up.shape[1]), f32)
-        block = pl.ds(pl.multiple_of(g * rows, rows), rows)
-        x = jnp.concatenate([arrived[part, block] for part in range(tp)], axis=1)
+        @pl.when(g == 0)
+        def _():
+            for xx in range(chips):
+                fn_copy(xx).wait_recv()
+
+        def one(k):
+            fp_copy(k).wait_recv()
+            for j in range(1, chips):
+                fq_copy(k, j).wait_recv()
+
+        over_group(g, one)
+        span = pl.ds(pl.multiple_of(g * rows, rows), rows)
+        x = jnp.concatenate([arrived[part, span] for part in range(tp)], axis=1)
         gate_act = jnp.dot(x, w_gate[...], preferred_element_type=f32)
         up_act = jnp.dot(x, w_up[...], preferred_element_type=f32)
         hidden = (jax.nn.silu(gate_act) * up_act).astype(bf16)
@@ -435,33 +485,33 @@
     def sum_step(g):
         for xx in range(chips):
             rs_copy(g, xx).wait_recv()
+        span = pl.ds(pl.multiple_of(g * rows, rows), rows)
         for j in range(1, chips):
             there = lax.rem(chip + j, chips)
-            rx_out[g, j - 1] = (rs_own[g, there].astype(f32) + rs_in[g, there].astype(f32)).astype(
-                bf16
-            )
-            rx_copy(g, j).start()
+            rx_out[j - 1, span] = (
+                rs_own[g, there].astype(f32) + rs_in[g, there].astype(f32)
+            ).astype(bf16)
+
+        def one(k):
+            for j in range(1, chips):
+                rx_copy(k, j).start()
+
+        over_group(g, one, 0)
 
     def return_step(g):
-        result = rs_own[g, chip].astype(f32) + rs_in[g, chip].astype(f32)
-        for j in range(1, chips):
-            rx_copy(g, j).wait_recv()
-            result = result + rx_in[g, j - 1].astype(f32)
-        result = result.astype(bf16)
-        answer[pl.ds(pl.multiple_of(g * rows, rows), rows), :] = result
-
-        @pl.when(g == 0)
-        def _():
-            returned[0:cap, :] = result[0:cap]
-
-        def give(k, _):
+        def one(k):
+            inner = pl.ds(pl.multiple_of((k - g * group) * cap, cap), cap)
+            result = rs_own[g, chip, inner].astype(f32) + rs_in[g, chip, inner].astype(f32)
+            for j in range(1, chips):
+                rx_copy(k, j).wait_recv()
+                result = result + rx_in[j - 1, block(k)].astype(f32)
+            answer[block(k), :] = result.astype(bf16)
+
             @pl.when(k > 0)
             def _():
                 ret_copy(k).start()
 
-            return 0
-
-        lax.fori_loop(g * group, (g + 1) * group, give, 0)
+        over_group(g, one, 0)
 
     total[...] = jnp.zeros_like(total)
 
@@ -471,76 +521,112 @@
             def _():
                 ret_copy(k).wait_recv()
 
-            expert = lax.rem(me + k, n)
+            expert = toward(k)
             weight = jnp.where(ids_ref[:, 0:1] == expert, route_ref[:, 0:1], 0.0) + jnp.where(
                 ids_ref[:, 1:2] == expert, route_ref[:, 1:2], 0.0
             )
-            answers = returned[pl.ds(pl.multiple_of(k * cap, cap), cap), :]
+            answers = returned[block(k), :]
             total[...] += weight * jnp.dot(onehots[k], answers, preferred_element_type=f32)
             return 0
 
         lax.fori_loop(g * group, (g + 1) * group, take, 0)
 
+    def place_of(k, _):
+        expert = toward(k)
+        member = jnp.maximum(
+            (ids_ref[:, 0:1] == expert).astype(f32), (ids_ref[:, 1:2] == expert).astype(f32)
+        )
+        member = jnp.broadcast_to(member, (tokens, cap))
+        place = jnp.dot(below, member.astype(bf16), preferred_element_type=f32)
+        slot = lax.broadcasted_iota(jnp.int32, (tokens, cap), 1).astype(f32)
+        onehots[k] = jnp.where(place == slot, member, 0.0).astype(bf16)
+        return 0
+
     def step(g, _):
+        @pl.when(g < groups)
+        def _():
+            expert_step(g)
+
+        @pl.when(g < groups)
+        def _():
+            sum_step(g)
+
+        @pl.when(g + 1 < groups)
+        def _():
+            forward_second(g + 1)
+
+        @pl.when(g == groups)
+        def _():
+            lax.fori_loop(0, n, place_of, 0)
+
+        @pl.when((g >= 1) & (g < groups + 1))
+        def _():
+            return_step(g - 1)
+
+        @pl.when(g == 0)
+        def _():
+            mix_stage()
+
         @pl.when(g + 2 < groups)
         def _():
             forward_first(g + 2)
 
-        @pl.when(g + 1 < groups)
-        def _():
-            forward_second(g + 1)
-
-        @pl.when(g < groups)
-        def _():
-            expert_step(g)
-
-        @pl.when(g == 0)
-        def _():
-            mix_stage()
-
-        @pl.when((g >= 1) & (g < groups + 1))
-        def _():
-            sum_step(g - 1)
-
-        @pl.when((g >= 2) & (g < groups + 2))
-        def _():
-            return_step(g - 2)
-
-        @pl.when(g >= 3)
-        def _():
-            combine_step(g - 3)
-
-        return 0
-
-    lax.fori_loop(0, groups + 3, step, 0)
+        @pl.when(g == groups - 1)
+        def _():
+            for j in range(1, chips):
+                mix_x_copy(j, 0).start()
+                mix_x_copy(j, 1).start()
+
+        return 0
+
+    lax.fori_loop(0, groups + 1, step, 0)
+    returned[0:cap, :] = answer[0:cap, :]
+
+    def combine(g, _):
+        combine_step(g)
+        return 0
+
+    lax.fori_loop(0, groups, combine, 0)
     expert_ref[...] = total[...].astype(bf16)
 
     mixed = mix_own[chip].astype(f32) + mix_in[chip].astype(f32)
     for j in range(1, chips):
-        mix_x_copy(j).wait_recv()
+        mix_x_copy(j, 0).wait_recv()
+        mix_x_copy(j, 1).wait_recv()
         mixed = mixed + mix_x_in[j - 1].astype(f32)
     mixer_ref[...] = mixed.astype(bf16)
+
+    ret_copy(1).wait_send()
 
     def left(k, _):
         a2a_copy(k).wait_send()
         ret_copy(k).wait_send()
-        return 0
-
-    lax.fori_loop(1, n, left, 0)
+        fp_copy(k).wait_send()
+        for j in range(1, chips):
+            fx_copy(k, j).wait_send()
+            fq_copy(k, j).wait_send()
+        return 0
+
+    lax.fori_loop(2, n, left, 0)
+
+    def left_x(k, _):
+        for j in range(1, chips):
+            rx_copy(k, j).wait_send()
+        return 0
+
+    lax.fori_loop(0, n, left_x, 0)
     halo_copy.wait_send()
     for j in range(1, tp):
         stat_copy(j).wait_send()
     for xx in range(chips):
         mix_copy(xx).wait_send()
+        near_copy(xx).wait_send()
+        fn_copy(xx).wait_send()
     for j in range(1, chips):
-        mix_x_copy(j).wait_send()
+        mix_x_copy(j, 0).wait_send()
+        mix_x_copy(j, 1).wait_send()
 
     def left_group(g, _):
-        fp_copy(g).wait_send()
-        for j in range(1, chips):
-            fx_copy(g, j).wait_send()
-            fq_copy(g, j).wait_send()
-            rx_copy(g, j).wait_send()
         for xx in range(chips):
             rs_copy(g, xx).wait_send()
         return 0
@@ -597,17 +683,23 @@
             V((width, hidden), bf16),
             V((hidden, width), bf16),
             dma((6,)),
+            V((tokens, width), bf16),
             V((n * cap, quarter), bf16),
+            V((chips, cap, quarter), bf16),
             V((n, tokens, cap), bf16),
             V((tp, n * cap, quarter), bf16),
+            dma((chips,)),
+            dma((chips,)),
+            dma((chips,)),
+            dma((chips,)),
             dma((n,)),
             dma((n,)),
-            dma((groups, others)),
-            dma((groups, others)),
-            dma((groups,)),
-            dma((groups,)),
-            dma((groups, others)),
-            dma((groups, others)),
+            dma((n, others)),
+            dma((n, others)),
+            dma((n,)),
+            dma((n,)),
+            dma((n, others)),
+            dma((n, others)),
             V((length, chan), bf16),
             V((halo, chan), bf16),
             dma,
@@ -626,17 +718,17 @@
             dma((chips,)),
             V((others, own_rows, out_weight.shape[1]), bf16),
             V((others, own_rows, out_weight.shape[1]), bf16),
-            dma((others,)),
-            dma((others,)),
+            dma((others, 2)),
+            dma((others, 2)),
             V((groups, chips, rows, quarter), bf16),
             V((groups, chips, rows, quarter), bf16),
             V((groups, chips, rows, quarter), bf16),
             dma((groups, chips)),
             dma((groups, chips)),
-            V((groups, others, rows, quarter), bf16),
-            V((groups, others, rows, quarter), bf16),
-            dma((groups, others)),
-            dma((groups, others)),
+            V((others, n * cap, quarter), bf16),
+            V((others, n * cap, quarter), bf16),
+            dma((n, others)),
+            dma((n, others)),
             V((n * cap, quarter), bf16),
             V((n * cap, quarter), bf16),
             dma((n,)),

time: 107 us -> 97.5 us (0.911)
  the two profiles are of different devices: /device:TPU:8 before, /device:TPU:16 now
where the time goes in v2:
time: 97.5 us; the launch traced here: 97.3 us
  Pallas kernels  90.1 us (92%)
  local copies, waits for them, and re-layouts  6.5 us (7%)
    pallas_call x1, Pallas kernels, on_device(): pl.pallas_call(functools.partial(kernel, n, tp, cap, group, reach), out_s...  90.1 us
    unnamed x4, local copies, waits for them, and re-layouts  6.5 us

profile of v2, /device:TPU:16, one launch (start us, length us, event | category | flops | bytes accessed | tf_op | source)
XLA Modules:
  0.0 97.3 jit_solution(7988686204918951980)
XLA Ops:
  0.6 1.5 %copy.15.route_ref = f32[256,2]{1,0:T(8,128)} copy(f32[256,2]{0,1:T(2,128)} %param.23) | data formatting | bytes 4096 | tf_op args[11]
  2.1 1.5 %copy.14.ids_ref = s32[256,2]{1,0:T(8,128)} copy(s32[256,2]{0,1:T(2,128)} %param.22) | data formatting | bytes 4096 | tf_op args[10]
  3.6 90.1 %block.1 = (bf16[128,2048]{1,0:T(8,128)(2,1)}, bf16[256,512]{1,0:T(8,128)(2,1)}) custom-call(bf16[256,2048]{1,0:T(8,128)(2,1)} %moe_ref.1, f32[1,2048]{1,0:T(1,128)} %bitcast.3, s32[256,2]{1,0:T(8,128)} %copy.14.ids_ref, s32[2,256]{1,0:T(2,128)} %bitcast.4, f32[256,2]{1,0:T(8,128)} %copy.15.route_ref, f32[31,256]{1,0:T(8,128)} %taps_ref.1, ...), custom_call_target="tpu_custom_call" | custom-call | tf_op jit(solution)/shard_map/block/pallas_call | solution.py:670
  93.7 1.9 %copy.18 = bf16[128,2048]{1,0:T(8,128)(2,1)} copy(bf16[128,2048]{1,0:T(8,128)(2,1)} %get-tuple-element.4) | data formatting | bytes 1048576
  95.6 1.7 %copy.19 = bf16[256,512]{1,0:T(8,128)(2,1)} copy(bf16[256,512]{1,0:T(8,128)(2,1)} %get-tuple-element.5) | data formatting | bytes 524288
